TPU v7x, 32 devices: a whole 2x2x4 slice. The times are simulated.
32 devices in a mesh: fs: 8 (over z, y), tp: 4 (over x, core).
Axes of the slice: x: 2, y: 2, z: 4, core: 2. Of those that a mesh axis runs over, the one named last changes fastest.
Arguments:
- inputs: bfloat16 [4608, 2048], P('fs'), may hold values from -6 to 6
- query_cotangent: bfloat16 [4608, 1024], P('fs', 'tp'), may hold values from -0.017944336 to 0.017944336
- value_cotangent: bfloat16 [4608, 1024], P('fs', 'tp'), may hold values from -0.017944336 to 0.017944336
- weights_query: float32 [2048, 1024], P('fs', 'tp'), may hold values from -6 to 6
- weights_value: float32 [2048, 1024], P('fs', 'tp'), may hold values from -6 to 6
- basis_query: bfloat16 [1024, 32], P('tp'), may hold values from -0.75 to 0.75
- basis_value: bfloat16 [1024, 32], P('tp'), may hold values from -0.75 to 0.75
- first_query: float32 [2048, 512], P('fs', 'tp'), may hold values from -5.4 to 5.4, as said below
- second_query: float32 [2048, 512], P('fs', 'tp'), may hold values from 0.05 to 1
- first_value: float32 [2048, 512], P('fs', 'tp'), may hold values from -5.4 to 5.4, as said below
- second_value: float32 [2048, 512], P('fs', 'tp'), may hold values from 0.05 to 1
Outputs:
- step_query: float32 [2048, 1024], P('fs', 'tp')
- step_value: float32 [2048, 1024], P('fs', 'tp')
- new_query: float32 [2048, 1024], P('fs', 'tp')
- new_value: float32 [2048, 1024], P('fs', 'tp')
- copy_query: bfloat16 [2048, 1024], P(None, 'tp')
- copy_value: bfloat16 [2048, 1024], P(None, 'tp')
- moment_query: float32 [2048, 512], P('fs', 'tp')
- square_query: float32 [2048, 512], P('fs', 'tp')
- moment_value: float32 [2048, 512], P('fs', 'tp')
- square_value: float32 [2048, 512], P('fs', 'tp')
Inputs may be any that keep to these rules, and one draw needn't show every extreme that they name: `first_query`: first moments, with a spread of scale from row to row. `first_value`: first moments, with a spread of scale from row to row.
All inputs are finite; a program needn't handle non-finite values.
Results may differ from a plain program's by a relative error of at most 0.003.
Values may be sent and summed in bfloat16 or wider, within the bound.
A program may use at most 64 MiB of HBM per device.

v0:
```python
import jax
import jax.numpy as jnp
from jax import lax
from jax.sharding import PartitionSpec as P

D = 2048
HEADS = 16
HEAD = 64
RK = 32


def from_space(direction, factor, heads_here):
    count = direction.shape[0]
    split = direction.reshape(count, heads_here, RK)
    out = jnp.einsum("nhr,hdr->nhd", split, factor, precision=lax.Precision.HIGHEST)
    return out.reshape(count, heads_here * HEAD)


def moments(reduced, first, second):
    moment = 0.9 * first + 0.1 * reduced
    square = 0.95 * second + 0.05 * reduced * reduced
    direction = moment / (jnp.sqrt(square) + 1e-08)
    return (moment, square, direction)


def per_device(
    inputs,
    query_cotangent,
    value_cotangent,
    weights_query,
    weights_value,
    basis_query,
    basis_value,
    first_query,
    second_query,
    first_value,
    second_value,
):
    own_cols = weights_query.shape[1]
    heads_here = own_cols // HEAD
    space_cols = heads_here * RK
    factor_q = basis_query.reshape(heads_here, HEAD, RK).astype(jnp.float32)
    factor_v = basis_value.reshape(heads_here, HEAD, RK).astype(jnp.float32)
    contract = (((0,), (0,)), ((), ()))
    tok_count = query_cotangent.shape[0]
    bf_q = basis_query.reshape(heads_here, HEAD, RK)
    bf_v = basis_value.reshape(heads_here, HEAD, RK)
    small_q = jnp.einsum(
        "thd,hdr->thr",
        query_cotangent.reshape(tok_count, heads_here, HEAD),
        bf_q,
        preferred_element_type=jnp.float32,
    )
    small_v = jnp.einsum(
        "thd,hdr->thr",
        value_cotangent.reshape(tok_count, heads_here, HEAD),
        bf_v,
        preferred_element_type=jnp.float32,
    )
    small_both = jnp.concatenate(
        (small_q.reshape(tok_count, space_cols), small_v.reshape(tok_count, space_cols)), axis=1
    )
    upper_part = small_both.astype(jnp.bfloat16)
    lower_part = (small_both - upper_part.astype(jnp.float32)).astype(jnp.bfloat16)
    high = lax.dot_general(inputs, upper_part, contract, preferred_element_type=jnp.float32)
    reduced = lax.psum_scatter(
        high + lax.dot_general(inputs, lower_part, contract, preferred_element_type=jnp.float32),
        "fs",
        scatter_dimension=0,
        tiled=True,
    )
    reduced_q = reduced[:, :space_cols]
    reduced_v = reduced[:, space_cols:]
    moment_q, square_q, direction_q = moments(reduced_q, first_query, second_query)
    moment_v, square_v, direction_v = moments(reduced_v, first_value, second_value)
    total_q, total_v = lax.psum(
        (jnp.sum(direction_q * direction_q), jnp.sum(direction_v * direction_v)), ("fs", "tp")
    )
    entries = D * HEADS * RK
    scale_q = 1.0 / jnp.sqrt(total_q / entries + 0.25)
    scale_v = 1.0 / jnp.sqrt(total_v / entries + 0.25)
    step_q = scale_q * from_space(direction_q, factor_q, heads_here)
    step_v = scale_v * from_space(direction_v, factor_v, heads_here)
    fresh_q = weights_query - 0.1 * step_q
    fresh_v = weights_value - 0.1 * step_v
    copy_q, copy_v = (
        lax.all_gather(fresh_q.astype(jnp.bfloat16), "fs", axis=0, tiled=True),
        lax.all_gather(fresh_v.astype(jnp.bfloat16), "fs", axis=0, tiled=True),
    )
    return (
        step_q,
        step_v,
        fresh_q,
        fresh_v,
        copy_q,
        copy_v,
        moment_q,
        square_q,
        moment_v,
        square_v,
    )


def solution(mesh):
    placed = (
        P("fs", None),
        P("fs", "tp"),
        P("fs", "tp"),
        P("fs", "tp"),
        P("fs", "tp"),
        P("tp", None),
        P("tp", None),
        P("fs", "tp"),
        P("fs", "tp"),
        P("fs", "tp"),
        P("fs", "tp"),
    )
    return jax.shard_map(
        per_device,
        mesh=mesh,
        in_specs=placed,
        out_specs=(
            P("fs", "tp"),
            P("fs", "tp"),
            P("fs", "tp"),
            P("fs", "tp"),
            P(None, "tp"),
            P(None, "tp"),
            P("fs", "tp"),
            P("fs", "tp"),
            P("fs", "tp"),
            P("fs", "tp"),
        ),
        check_vma=False,
    )
```

profile of v0, /device:TPU:0, one launch (start us, length us, event | category | flops | bytes accessed | tf_op | source)
XLA Modules:
  0.0 223.8 jit_solution(16746739006652718097)
XLA Ops:
  7.2 0.0 copy-start
  7.2 0.0 reduce-scatter.2.cloned.1.call-start
  7.2 1.0 reshape.52
  8.2 0.0 copy-start.4
  8.2 0.8 reshape.55
  9.0 1.2 copy.40
  10.2 1.2 copy.42
  11.4 0.2 fusion.10
  11.6 0.2 fusion.7
  11.7 0.0 copy-done
  11.8 1.0 fusion.2
  12.8 0.0 copy-done.4
  12.8 0.0 copy-start.5
  12.8 2.3 %fusion = f32[2048,256]{0,1:T(8,128)} fusion(f32[256,2048]{1,0:T(8,128)S(1)} %fusion.2, bf16[576,2048]{1,0:T(8,128)(2,1)S(1)} %copy-done, f32[576,128]{0,1:T(8,128)S(1)} %bitcast.31, f32[576,128]{0,1:T(8,128)S(1)} %bitcast.29), kind=kOutput, calls=%fused_computation.1 | convolution fusion | flops 605241344 | bytes 7143424 | tf_op jit(solution)/shard_map/dot_general | solution.py:67
  15.1 0.0 copy-start.6
  15.1 0.0 copy-start.7
  15.1 0.0 copy-start.8
  15.1 0.0 reduce-scatter.2.cloned.1.call-update
  15.2 0.0 all-gather.5.cloned.1.call-start
  15.2 0.0 copy-done.5
  15.2 0.1 copy.39
  15.3 0.7 copy-done.6
  16.0 0.1 copy.44
  16.1 0.0 copy-done.7
  16.1 0.1 copy.46
  16.3 0.0 copy-done.8
  16.3 0.1 copy.47
  16.4 70.6 %reduce-scatter.2.cloned.1.call-done = f32[256,256]{0,1:T(8,128)} async-done(((f32[2048,256]{0,1:T(8,128)}), f32[256,256]{0,1:T(8,128)}) %reduce-scatter.2.cloned.1.call-update) | async-done | bytes 262160 | tf_op jit(solution)/shard_map/reduce_scatter | solution.py:66
  86.9 2.4 %multiply_reduce_fusion = (f32[]{:T(128)}, f32[256,128]{0,1:T(8,128)S(1)}, f32[256,128]{0,1:T(8,128)}, f32[256,128]{0,1:T(8,128)S(1)}, f32[]{:T(128)}, /*index=5...) fusion(f32[256,256]{0,1:T(8,128)} %reduce-scatter.2.cloned.1.call-done, f32[256,128]{0,1:T(8,128)S(1)} %copy.47, ...), kind=kLoop, calls=%fused_computation.14 | loop fusion | flops 720894 | bytes 1572872 | tf_op jit(solution)/shard_map/reduce_sum | solution.py:77
  89.3 39.8 %all-reduce = (f32[]{:T(128)}, f32[]{:T(128)}) all-reduce(f32[]{:T(128)} %get-tuple-element.44, f32[]{:T(128)} %get-tuple-element.36), channel_id=1, replica_groups=mesh['fs'=8,'tp'=4] {'fs','tp'}, use_global_device_ids=true, to_apply=%region_2.0 | all-reduce | flops 2 | bytes 16 | tf_op jit(solution)/shard_map/psum | solution.py:76
  129.8 0.3 convolution_multiply_fusion
  130.1 0.1 copy.52
  130.3 0.0 copy-start.1
  130.3 1.8 fusion.14
  132.1 0.0 all-gather.5.cloned.1.call-update
  132.1 0.0 all-gather.3.cloned.1.call-start
  132.9 1.2 convolution_multiply_fusion.1
  134.1 0.1 copy.51
  134.2 0.0 copy-start.2
  134.2 1.8 fusion.15
  136.1 0.0 all-gather.3.cloned.1.call-update
  136.1 1.7 copy.56
  137.8 0.8 copy.55
  138.5 0.8 copy.54
  139.3 0.8 copy.53
  140.0 32.2 %all-gather.5.cloned.1.call-done = bf16[2048,256]{1,0:T(8,128)(2,1)} async-done(((bf16[256,256]{1,0:T(8,128)(2,1)}), bf16[2048,256]{1,0:T(8,128)(2,1)}) %all-gather.5.cloned.1.call-update) | async-done | bytes 1048592 | tf_op jit(solution)/shard_map/all_gather | solution.py:88
  172.3 41.7 %all-gather.3.cloned.1.call-done = bf16[2048,256]{1,0:T(8,128)(2,1)} async-done(((bf16[256,256]{1,0:T(8,128)(2,1)}), bf16[2048,256]{1,0:T(8,128)(2,1)}) %all-gather.3.cloned.1.call-update) | async-done | bytes 1048592 | tf_op jit(solution)/shard_map/all_gather | solution.py:87
  214.0 0.0 copy-start.3
  214.0 2.4 %copy.67 = bf16[2048,256]{1,0:T(8,128)(2,1)} copy(bf16[2048,256]{1,0:T(8,128)(2,1)} %all-gather.3.cloned.1.call-done) | data formatting | bytes 2097152
  216.3 0.0 copy-done.1
  216.3 0.0 copy-done.3
  216.3 1.0 copy.68
  217.3 0.0 copy-done.2
Async XLA Ops:
  7.2 4.6 %copy-start = (bf16[576,2048]{1,0:T(8,128)(2,1)S(1)}, bf16[576,2048]{1,0:T(8,128)(2,1)}, u32[]{:S(2)}) copy-start(bf16[576,2048]{1,0:T(8,128)(2,1)} %param.11) | copy-start | bytes 7077892
  7.2 79.7 %reduce-scatter.2.cloned.1.call-start = ((), (), s32[]{:S(2)}) async-start(), calls=%async_computation.1 | async-start | bytes 2359296 | tf_op jit(solution)/shard_map/reduce_scatter | solution.py:66
  8.2 4.6 %copy-start.4 = (bf16[4,64,32]{1,0,2:T(4,128)(2,1)}, bf16[4,64,32]{1,0,2:T(4,128)(2,1)S(1)}, u32[]{:S(2)}) copy-start(bf16[4,64,32]{1,0,2:T(4,128)(2,1)S(1)} %reshape.52) | copy-start | bytes 49156
  12.8 2.4 %copy-start.5 = (f32[256,128]{1,0:T(8,128)S(1)}, f32[256,128]{1,0:T(8,128)}, u32[]{:S(2)}) copy-start(f32[256,128]{1,0:T(8,128)} %param.18) | copy-start | bytes 393220
  15.1 0.9 copy-start.6
  15.1 1.0 copy-start.7
  15.1 1.1 copy-start.8
  15.2 157.1 %all-gather.5.cloned.1.call-start = ((), (), s32[]{:S(2)}) async-start(), calls=%async_computation.3 | async-start | bytes 1179648 | tf_op jit(solution)/shard_map/all_gather | solution.py:88
  130.3 86.1 %copy-start.1 = (f32[256,256]{1,0:T(8,128)}, f32[256,256]{1,0:T(8,128)S(1)}, u32[]{:S(2)}) copy-start(f32[256,256]{1,0:T(8,128)S(1)} %copy.52) | copy-start | bytes 786436
  132.1 81.8 %all-gather.3.cloned.1.call-start = ((), (), s32[]{:S(2)}) async-start(), calls=%async_computation.2 | async-start | bytes 1179648 | tf_op jit(solution)/shard_map/all_gather | solution.py:87
  134.2 83.1 %copy-start.2 = (f32[256,256]{1,0:T(8,128)}, f32[256,256]{1,0:T(8,128)S(1)}, u32[]{:S(2)}) copy-start(f32[256,256]{1,0:T(8,128)S(1)} %copy.51) | copy-start | bytes 786436
  214.0 2.4 %copy-start.3 = (bf16[2048,256]{1,0:T(8,128)(2,1)S(1)}, bf16[2048,256]{1,0:T(8,128)(2,1)}, u32[]{:S(2)}) copy-start(bf16[2048,256]{1,0:T(8,128)(2,1)} %all-gather.5.cloned.1.call-done) | copy-start | bytes 3145732
Sparse Core Ops, SparseCore 0:
  15.3 71.6 reduce-scatter.1
  132.3 39.9 all-gather.4
  175.0 38.9 all-gather.2
where the time goes:
time: 224 us
  waiting for transfers between devices  145 us (65%)
  blocking collectives  39.8 us (18%)
  between operations  15.3 us (7%)
  local copies, waits for them, and re-layouts  12.7 us (6%)
  other arithmetic  6.06 us (3%)
  matrix products  5.25 us (2%)
    reduce_scatter x1, waiting for transfers between devices, per_device(): lax.psum_scatter(high + lax.dot_general(inputs, lower_part, contract, pre...  70.6 us
    all_gather x1, waiting for transfers between devices, per_device(): lax.all_gather(fresh_q.astype(jnp.bfloat16), 'fs', axis=0, tiled=True)  41.7 us
    psum x1, blocking collectives, per_device(): lax.psum((jnp.sum(direction_q * direction_q), jnp.sum(direction_v * direc...  39.8 us
    all_gather x1, waiting for transfers between devices, per_device(): lax.all_gather(fresh_v.astype(jnp.bfloat16), 'fs', axis=0, tiled=True)  32.2 us
    unnamed x32, local copies, waits for them, and re-layouts  11 us
  transfers between devices with their start and end apart: 3, of which 3 were waited for; matrix products, arithmetic and copies ran while one was open for 3% of the time, Pallas kernels for 0%

commit v1 on v0

--- a/solution.py
+++ b/solution.py
@@ -74,7 +74,8 @@
     moment_q, square_q, direction_q = moments(reduced_q, first_query, second_query)
     moment_v, square_v, direction_v = moments(reduced_v, first_value, second_value)
     total_q, total_v = lax.psum(
-        (jnp.sum(direction_q * direction_q), jnp.sum(direction_v * direction_v)), ("fs", "tp")
+        lax.psum((jnp.sum(direction_q * direction_q), jnp.sum(direction_v * direction_v)), "tp"),
+        "fs",
     )
     entries = D * HEADS * RK
     scale_q = 1.0 / jnp.sqrt(total_q / entries + 0.25)

time: 224 us -> 208 us (0.929)
  blocking collectives: 39.8 us -> 26 us
  waiting for transfers between devices: 145 us -> 142 us
    psum x1, blocking collectives: 39.8 us -> 6.27 us  [per_device(): lax.psum((jnp.sum(direction_q * direction_q), jnp.sum(direction_v * direc...]
    psum x0 -> x1, blocking collectives: none -> 19.7 us  [per_device(): lax.psum(lax.psum((jnp.sum(direction_q * direction_q), jnp.sum(direction_...]
  transfers between devices with their start and end apart: 3 -> 3, of which waited for: 3 -> 3; matrix products, arithmetic and copies ran while one was open for 3% -> 4% of each run, Pallas kernels for 0% -> 0%
where the time goes in v1:
time: 208 us
  waiting for transfers between devices  142 us (68%)
  blocking collectives  26 us (12%)
  between operations  15.3 us (7%)
  local copies, waits for them, and re-layouts  12.7 us (6%)
  other arithmetic  6.06 us (3%)
  matrix products  5.26 us (3%)
    reduce_scatter x1, waiting for transfers between devices, per_device(): lax.psum_scatter(high + lax.dot_general(inputs, lower_part, contract, pre...  70.6 us
    all_gather x1, waiting for transfers between devices, per_device(): lax.all_gather(fresh_q.astype(jnp.bfloat16), 'fs', axis=0, tiled=True)  41.7 us
    all_gather x1, waiting for transfers between devices, per_device(): lax.all_gather(fresh_v.astype(jnp.bfloat16), 'fs', axis=0, tiled=True)  30 us
    psum x1, blocking collectives, per_device(): lax.psum(lax.psum((jnp.sum(direction_q * direction_q), jnp.sum(direction_...  19.7 us
    unnamed x32, local copies, waits for them, and re-layouts  11 us
    psum x1, blocking collectives, per_device(): lax.psum((jnp.sum(direction_q * direction_q), jnp.sum(direction_v * direc...  6.27 us
  transfers between devices with their start and end apart: 3, of which 3 were waited for; matrix products, arithmetic and copies ran while one was open for 4% of the time, Pallas kernels for 0%

profile of v1, /device:TPU:0, one launch (start us, length us, event | category | flops | bytes accessed | tf_op | source)
XLA Modules:
  0.0 207.9 jit_solution(15692261895530256214)
XLA Ops:
  7.2 0.0 copy-start
  7.2 0.0 reduce-scatter.2.cloned.1.call-start
  7.2 1.0 reshape.52
  8.2 0.0 copy-start.4
  8.2 0.8 reshape.55
  9.0 1.2 copy.40
  10.2 1.2 copy.42
  11.4 0.2 fusion.10
  11.6 0.2 fusion.7
  11.7 0.0 copy-done
  11.8 1.0 fusion.2
  12.8 0.0 copy-done.4
  12.8 0.0 copy-start.5
  12.8 2.4 %fusion = f32[2048,256]{0,1:T(8,128)} fusion(f32[256,2048]{1,0:T(8,128)S(1)} %fusion.2, bf16[576,2048]{1,0:T(8,128)(2,1)S(1)} %copy-done, f32[576,128]{0,1:T(8,128)S(1)} %bitcast.31, f32[576,128]{0,1:T(8,128)S(1)} %bitcast.29), kind=kOutput, calls=%fused_computation.1 | convolution fusion | flops 605241344 | bytes 7143424 | tf_op jit(solution)/shard_map/dot_general | solution.py:67
  15.1 0.0 copy-start.6
  15.1 0.0 copy-start.7
  15.1 0.0 copy-start.8
  15.1 0.0 reduce-scatter.2.cloned.1.call-update
  15.2 0.0 all-gather.5.cloned.1.call-start
  15.2 0.0 copy-done.5
  15.2 0.1 copy.39
  15.3 0.7 copy-done.6
  16.0 0.1 copy.44
  16.1 0.0 copy-done.7
  16.2 0.1 copy.46
  16.3 0.0 copy-done.8
  16.3 0.1 copy.47
  16.4 70.6 %reduce-scatter.2.cloned.1.call-done = f32[256,256]{0,1:T(8,128)} async-done(((f32[2048,256]{0,1:T(8,128)}), f32[256,256]{0,1:T(8,128)}) %reduce-scatter.2.cloned.1.call-update) | async-done | bytes 262160 | tf_op jit(solution)/shard_map/reduce_scatter | solution.py:66
  86.9 2.4 %multiply_reduce_fusion = (f32[]{:T(128)}, f32[256,128]{0,1:T(8,128)S(1)}, f32[256,128]{0,1:T(8,128)}, f32[256,128]{0,1:T(8,128)S(1)}, f32[]{:T(128)}, /*index=5...) fusion(f32[256,256]{0,1:T(8,128)} %reduce-scatter.2.cloned.1.call-done, f32[256,128]{0,1:T(8,128)S(1)} %copy.47, ...), kind=kLoop, calls=%fused_computation.14 | loop fusion | flops 720894 | bytes 1572872 | tf_op jit(solution)/shard_map/reduce_sum | solution.py:77
  89.4 6.3 %all-reduce.1 = (f32[]{:T(128)}, f32[]{:T(128)}) all-reduce(f32[]{:T(128)} %get-tuple-element.46, f32[]{:T(128)} %get-tuple-element.38), channel_id=1, replica_groups=mesh['fs'=8,'tp'=4] {'tp'}, use_global_device_ids=true, to_apply=%region_2.0 | all-reduce | flops 2 | bytes 16 | tf_op jit(solution)/shard_map/psum | solution.py:77
  95.6 19.7 %all-reduce = (f32[]{:T(128)}, f32[]{:T(128)}) all-reduce(f32[]{:T(128)} %get-tuple-element.32, f32[]{:T(128)} %get-tuple-element.33), channel_id=1, replica_groups=mesh['fs'=8,'tp'=4] {'fs'}, use_global_device_ids=true, to_apply=%region_3.0 | all-reduce | flops 2 | bytes 16 | tf_op jit(solution)/shard_map/psum | solution.py:76
  116.0 0.3 convolution_multiply_fusion
  116.4 0.1 copy.52
  116.5 0.0 copy-start.1
  116.5 1.8 fusion.14
  118.3 0.0 all-gather.5.cloned.1.call-update
  118.4 0.0 all-gather.3.cloned.1.call-start
  119.1 1.2 convolution_multiply_fusion.1
  120.3 0.1 copy.51
  120.5 0.0 copy-start.2
  120.5 1.8 fusion.15
  122.3 0.0 all-gather.3.cloned.1.call-update
  122.3 1.7 copy.56
  124.0 0.8 copy.55
  124.7 0.8 copy.54
  125.5 0.8 copy.53
  126.2 30.0 %all-gather.5.cloned.1.call-done = bf16[2048,256]{1,0:T(8,128)(2,1)} async-done(((bf16[256,256]{1,0:T(8,128)(2,1)}), bf16[2048,256]{1,0:T(8,128)(2,1)}) %all-gather.5.cloned.1.call-update) | async-done | bytes 1048592 | tf_op jit(solution)/shard_map/all_gather | solution.py:89
  156.3 41.7 %all-gather.3.cloned.1.call-done = bf16[2048,256]{1,0:T(8,128)(2,1)} async-done(((bf16[256,256]{1,0:T(8,128)(2,1)}), bf16[2048,256]{1,0:T(8,128)(2,1)}) %all-gather.3.cloned.1.call-update) | async-done | bytes 1048592 | tf_op jit(solution)/shard_map/all_gather | solution.py:88
  198.0 0.0 copy-start.3
  198.0 2.4 %copy.67 = bf16[2048,256]{1,0:T(8,128)(2,1)} copy(bf16[2048,256]{1,0:T(8,128)(2,1)} %all-gather.3.cloned.1.call-done) | data formatting | bytes 2097152
  200.4 0.0 copy-done.1
  200.4 0.0 copy-done.3
  200.4 1.0 copy.68
  201.3 0.0 copy-done.2
Async XLA Ops:
  7.2 4.6 %copy-start = (bf16[576,2048]{1,0:T(8,128)(2,1)S(1)}, bf16[576,2048]{1,0:T(8,128)(2,1)}, u32[]{:S(2)}) copy-start(bf16[576,2048]{1,0:T(8,128)(2,1)} %param.11) | copy-start | bytes 7077892
  7.2 79.8 %reduce-scatter.2.cloned.1.call-start = ((), (), s32[]{:S(2)}) async-start(), calls=%async_computation.1 | async-start | bytes 2359296 | tf_op jit(solution)/shard_map/reduce_scatter | solution.py:66
  8.2 4.6 %copy-start.4 = (bf16[4,64,32]{1,0,2:T(4,128)(2,1)}, bf16[4,64,32]{1,0,2:T(4,128)(2,1)S(1)}, u32[]{:S(2)}) copy-start(bf16[4,64,32]{1,0,2:T(4,128)(2,1)S(1)} %reshape.52) | copy-start | bytes 49156
  12.8 2.4 %copy-start.5 = (f32[256,128]{1,0:T(8,128)S(1)}, f32[256,128]{1,0:T(8,128)}, u32[]{:S(2)}) copy-start(f32[256,128]{1,0:T(8,128)} %param.18) | copy-start | bytes 393220
  15.1 0.9 copy-start.6
  15.1 1.0 copy-start.7
  15.1 1.1 copy-start.8
  15.2 141.1 %all-gather.5.cloned.1.call-start = ((), (), s32[]{:S(2)}) async-start(), calls=%async_computation.3 | async-start | bytes 1179648 | tf_op jit(solution)/shard_map/all_gather | solution.py:89
  116.5 83.9 %copy-start.1 = (f32[256,256]{1,0:T(8,128)}, f32[256,256]{1,0:T(8,128)S(1)}, u32[]{:S(2)}) copy-start(f32[256,256]{1,0:T(8,128)S(1)} %copy.52) | copy-start | bytes 786436
  118.4 79.7 %all-gather.3.cloned.1.call-start = ((), (), s32[]{:S(2)}) async-start(), calls=%async_computation.2 | async-start | bytes 1179648 | tf_op jit(solution)/shard_map/all_gather | solution.py:88
  120.5 80.9 %copy-start.2 = (f32[256,256]{1,0:T(8,128)}, f32[256,256]{1,0:T(8,128)S(1)}, u32[]{:S(2)}) copy-start(f32[256,256]{1,0:T(8,128)S(1)} %copy.51) | copy-start | bytes 786436
  198.0 2.4 %copy-start.3 = (bf16[2048,256]{1,0:T(8,128)(2,1)S(1)}, bf16[2048,256]{1,0:T(8,128)(2,1)}, u32[]{:S(2)}) copy-start(bf16[2048,256]{1,0:T(8,128)(2,1)} %all-gather.5.cloned.1.call-done) | copy-start | bytes 3145732
Sparse Core Ops, SparseCore 0:
  15.3 71.6 reduce-scatter.1
  118.5 37.7 all-gather.4
  159.0 38.9 all-gather.2
